TPU v7x, 32 devices: a whole 2x2x4 slice. The times are simulated.
32 devices in a mesh: ep: 8 (over z, y), tp: 4 (over x, core).
Axes of the slice: x: 2, y: 2, z: 4, core: 2. Of those that a mesh axis runs over, the one named last changes fastest.
Arguments:
- tokens: bfloat16 [2048, 1024], P('ep'), may hold values from -6 to 6
- cotangent: bfloat16 [2048, 1024], P('ep'), may hold values from -1.5 to 1.5
- routing: int32 [2048, 2], P('ep'), may hold values from 0 to 15, all different within a row; in each aligned block of 256 rows (0 to 255, 256 to 511, ...) at most 96 rows name the same one
- gate_weights: float32 [2048, 2], P('ep'), may hold values from 0.1 to 0.9
- gate_proj: bfloat16 [16, 1024, 512], P('ep', None, 'tp'), may hold values from -0.1875 to 0.1875
- up_proj: bfloat16 [16, 1024, 512], P('ep', None, 'tp'), may hold values from -0.1875 to 0.1875
- down_proj: bfloat16 [16, 512, 1024], P('ep', 'tp'), may hold values from -0.25 to 0.25
Outputs:
- tokens_grad: bfloat16 [2048, 1024], P('ep')
- gates_grad: float32 [2048, 2], P('ep')
- gate_proj_grad: float32 [16, 1024, 512], P('ep', None, 'tp')
- up_proj_grad: float32 [16, 1024, 512], P('ep', None, 'tp')
- down_proj_grad: float32 [16, 512, 1024], P('ep', 'tp')
Inputs may be any that keep to these rules, and one draw needn't show every extreme that they name: `routing`: each row names 2 different experts; every expert is named by some row; within each aligned block of 256 rows (the tokens of one index of ep) no expert is named by more than 96 rows, a bound that some block reaches.
All inputs are finite; a program needn't handle non-finite values.
Results may differ from a plain program's by a relative error of at most 0.0015.
Values may be sent and summed in bfloat16 or wider, within the bound.
A program may use at most 128 MiB of HBM per device.

v0:
```python
import jax
import jax.numpy as jnp
from jax import lax
from jax.sharding import PartitionSpec as P


def expert_terms(expert_rows, expert_scaled, gate_proj, up_proj, down_proj):
    gate_pre = jnp.einsum(
        "erd,edf->erf", expert_rows, gate_proj, preferred_element_type=jnp.float32
    ).astype(jnp.bfloat16)
    up_pre = jnp.einsum(
        "erd,edf->erf", expert_rows, up_proj, preferred_element_type=jnp.float32
    ).astype(jnp.bfloat16)
    gate_pre, up_pre = lax.optimization_barrier((gate_pre, up_pre))
    hidden_grad = jnp.einsum(
        "erd,efd->erf", expert_scaled, down_proj, preferred_element_type=jnp.float32
    )
    gate_wide = gate_pre.astype(jnp.float32)
    up_wide = up_pre.astype(jnp.float32)
    sigmoid_gate = jax.nn.sigmoid(gate_wide)
    activated = gate_wide * sigmoid_gate
    hidden = activated * up_wide
    product = jnp.sum(hidden_grad * hidden, axis=-1)
    gate_pre_grad = (
        hidden_grad * up_wide * sigmoid_gate * (1.0 + gate_wide * (1.0 - sigmoid_gate))
    ).astype(jnp.bfloat16)
    up_pre_grad = (hidden_grad * activated).astype(jnp.bfloat16)
    input_grad = jnp.einsum(
        "erf,edf->erd", gate_pre_grad, gate_proj, preferred_element_type=jnp.float32
    )
    input_grad = input_grad + jnp.einsum(
        "erf,edf->erd", up_pre_grad, up_proj, preferred_element_type=jnp.float32
    )
    down_grad = jnp.einsum(
        "erf,erd->efd",
        hidden.astype(jnp.bfloat16),
        expert_scaled,
        preferred_element_type=jnp.float32,
    )
    gate_grad = jnp.einsum(
        "erd,erf->edf", expert_rows, gate_pre_grad, preferred_element_type=jnp.float32
    )
    up_grad = jnp.einsum(
        "erd,erf->edf", expert_rows, up_pre_grad, preferred_element_type=jnp.float32
    )
    return (input_grad, product, gate_grad, up_grad, down_grad)


def shards(tokens, cotangent, routing, gate_weights, gate_proj, up_proj, down_proj):
    token_count, model_width = tokens.shape
    top_count = routing.shape[1]
    local_experts = gate_proj.shape[0]
    groups = lax.axis_size("ep")
    members = lax.axis_size("tp")
    experts = local_experts * groups
    capacity = members * (
        (3 * token_count * top_count + experts * members - 1) // (experts * members)
    )
    slot_count = experts * capacity
    pair_count = token_count * top_count
    pair_expert = routing.reshape(pair_count)
    onehot = (pair_expert[:, None] == jnp.arange(experts, dtype=jnp.int32)[None, :]).astype(
        jnp.int32
    )
    position = jnp.sum(jnp.cumsum(onehot, axis=0) * onehot, axis=1) - 1
    pair_slot = pair_expert * capacity + position
    pair_number = jnp.arange(pair_count, dtype=jnp.int32)
    owner_pair = jnp.zeros((slot_count,), jnp.int32).at[pair_slot].set(pair_number)
    filled = jnp.zeros((slot_count,), jnp.int32).at[pair_slot].set(1) > 0
    owner_token = owner_pair // top_count
    slot_weight = jnp.where(filled, gate_weights.reshape(pair_count)[owner_pair], 0.0)
    send_rows = jnp.where(filled[:, None], tokens[owner_token], jnp.zeros((), jnp.bfloat16))
    send_scaled = (slot_weight[:, None] * cotangent[owner_token].astype(jnp.float32)).astype(
        jnp.bfloat16
    )
    layout = (groups, local_experts, capacity, model_width)
    send_rows = send_rows.reshape(layout)
    send_scaled = send_scaled.reshape(layout)
    quarter = capacity // members
    quarter_start = lax.axis_index("tp") * quarter
    part_rows = lax.dynamic_slice_in_dim(send_rows, quarter_start, quarter, 2)
    part_scaled = lax.dynamic_slice_in_dim(send_scaled, quarter_start, quarter, 2)
    landed = (
        lax.all_to_all(part_rows, "ep", split_axis=0, concat_axis=0, tiled=True),
        lax.all_to_all(part_scaled, "ep", split_axis=0, concat_axis=0, tiled=True),
    )
    recv_rows, recv_scaled = (
        lax.all_gather(landed[0], "tp", axis=2, tiled=True),
        lax.all_gather(landed[1], "tp", axis=2, tiled=True),
    )
    expert_rows = recv_rows.transpose(1, 0, 2, 3).reshape(
        local_experts, groups * capacity, model_width
    )
    expert_scaled = recv_scaled.transpose(1, 0, 2, 3).reshape(
        local_experts, groups * capacity, model_width
    )
    input_grad, product, gate_grad, up_grad, down_grad = expert_terms(
        expert_rows, expert_scaled, gate_proj, up_proj, down_proj
    )
    input_grad = input_grad.reshape(local_experts, groups, capacity, model_width).transpose(
        1, 0, 2, 3
    )
    product = product.reshape(local_experts, groups, capacity).transpose(1, 0, 2)
    back_grad, back_product = (
        lax.all_to_all(input_grad, "ep", split_axis=0, concat_axis=0, tiled=True),
        lax.all_to_all(product, "ep", split_axis=0, concat_axis=0, tiled=True),
    )
    local_slot = position
    present = (local_slot >= 0) & (local_slot < capacity)
    back_index = pair_expert * capacity + jnp.clip(local_slot, 0, capacity - 1)
    pair_grad = jnp.where(
        present[:, None], back_grad.reshape(experts * capacity, model_width)[back_index], 0.0
    )
    pair_product = jnp.where(present, back_product.reshape(experts * capacity)[back_index], 0.0)
    token_grad = jnp.sum(pair_grad.reshape(token_count, top_count, model_width), axis=1)
    total_grad, total_product = lax.psum((token_grad, pair_product), "tp")
    tokens_grad = total_grad.astype(jnp.bfloat16)
    gates_grad = (total_product / gate_weights.reshape(pair_count)).reshape(token_count, top_count)
    return (tokens_grad, gates_grad, gate_grad, up_grad, down_grad)


def solution(mesh):
    in_specs = (
        P("ep", None),
        P("ep", None),
        P("ep", None),
        P("ep", None),
        P("ep", None, "tp"),
        P("ep", None, "tp"),
        P("ep", "tp", None),
    )
    out_specs = (
        P("ep", None),
        P("ep", None),
        P("ep", None, "tp"),
        P("ep", None, "tp"),
        P("ep", "tp", None),
    )
    return jax.shard_map(shards, mesh=mesh, in_specs=in_specs, out_specs=out_specs, check_vma=False)
```

profile of v0, /device:TPU:0, one launch (start us, length us, event | category | flops | bytes accessed | tf_op | source)
XLA Modules:
  0.0 324.4 jit_solution(3575784898565409781)
XLA Ops:
  9.4 1.2 reduce-window.6
  10.9 2.5 scatter_custom_fusion.1
  13.4 2.5 scatter_custom_fusion
  15.9 0.8 copy.66
  16.9 9.5 %gather_fusion = f32[1536]{0:T(1024)S(1)} fusion(f32[512]{0:T(512)S(1)} %reshape.148, s32[2048]{0:T(1024)S(1)} %get-tuple-element.38), kind=kCustom, calls=%fused_computation | custom fusion | bytes 18432 | tf_op jit(solution)/shard_map/gather | solution.py:71
  26.5 5.8 %gather_fusion.2 = bf16[1536,1024]{1,0:T(8,128)(2,1)} fusion(bf16[256,1024]{1,0:T(8,128)(2,1)S(1)} %copy-done.1, s32[2048]{0:T(1024)S(1)} %get-tuple-element.37), kind=kCustom, calls=%fused_computation.2 | custom fusion | bytes 6297600 | tf_op jit(solution)/shard_map/gather | solution.py:72
  32.3 1.4 dynamic-slice_select_fusion
  33.7 27.4 %all_to_all.20 = bf16[8,2,24,1024]{3,2,1,0:T(8,128)(2,1)} all-to-all(bf16[8,2,24,1024]{3,2,1,0:T(8,128)(2,1)S(1)} %dynamic-slice_select_fusion), channel_id=1, replica_groups=mesh['ep'=8,'tp'=4] {'ep'}, dimensions={0} | all-to-all | bytes 1572864 | tf_op jit(solution)/shard_map/all_to_all | solution.py:84
  61.3 5.8 %gather_fusion.1 = bf16[1536,1024]{1,0:T(8,128)(2,1)} fusion(bf16[256,1024]{1,0:T(8,128)(2,1)S(1)} %copy-done.2, s32[2048]{0:T(1024)S(1)} %get-tuple-element.37), kind=kCustom, calls=%fused_computation.1 | custom fusion | bytes 6297600 | tf_op jit(solution)/shard_map/gather | solution.py:73
  67.1 1.4 fusion
  68.5 23.2 %all_to_all.21 = bf16[8,2,24,1024]{3,2,1,0:T(8,128)(2,1)} all-to-all(bf16[8,2,24,1024]{3,2,1,0:T(8,128)(2,1)S(1)} %fusion), channel_id=1, replica_groups=mesh['ep'=8,'tp'=4] {'ep'}, dimensions={0} | all-to-all | bytes 1572864 | tf_op jit(solution)/shard_map/all_to_all | solution.py:85
  91.8 2.4 copy.68
  94.2 1.2 convolution_convert_fusion
  95.9 1.2 convolution_convert_fusion.1
  97.1 22.4 %all-gather.3.cloned.1.call-done = bf16[8,2,96,1024]{3,2,1,0:T(8,128)(2,1)} async-done(((bf16[8,2,24,1024]{3,2,1,0:T(8,128)(2,1)}), bf16[8,2,96,1024]{3,2,1,0:T(8,128)(2,1)}) %all-gather.3.cloned.1.call-update) | async-done | bytes 3145744 | tf_op jit(solution)/shard_map/all_gather | solution.py:89
  119.5 2.4 copy.67
  121.9 1.4 multiply_reduce_fusion
  124.2 5.5 %all-to-all-start.3 = ((f32[8,2,96]{2,1,0:T(2,128)}), f32[8,2,96]{2,1,0:T(2,128)S(1)}, u32[]{:S(2)}, u32[]{:S(2)}) async-start(f32[8,2,96]{2,1,0:T(2,128)} %copy.74), calls=%async_computation.3 | async-start | bytes 16384 | tf_op jit(solution)/shard_map/all_to_all | solution.py:106
  129.7 1.0 fusion.21
  130.7 1.1 convolution_add_fusion
  131.8 3.2 copy.91
  135.1 1.2 all-to-all-done.3
  136.2 4.8 %all-to-all-start.2 = ((f32[8,2,96,1024]{3,2,1,0:T(8,128)}), f32[8,2,96,1024]{3,2,1,0:T(8,128)}, u32[]{:S(2)}, u32[]{:S(2)}) async-start(f32[8,2,96,1024]{3,2,1,0:T(8,128)} %bitcast.50), calls=%async_computation.2 | async-start | bytes 12582912 | tf_op jit(solution)/shard_map/all_to_all | solution.py:105
  141.1 4.4 %fusion.22 = f32[2,1024,128]{2,1,0:T(8,128)} fusion(bf16[2,768,1024]{2,1,0:T(8,128)(2,1)} %bitcast.48, bf16[2,768,128]{1,2,0:T(8,128)(2,1)S(1)} %get-tuple-element.31), kind=kOutput, calls=%fused_computation.67 | convolution fusion | flops 402653184 | bytes 4587520 | tf_op jit(solution)/shard_map/erd,erf->edf/dot_general | solution.py:40
  145.4 1.8 fusion.9
  147.7 2.4 fusion.20
  150.1 3.1 gather_fusion.4
  153.4 125.7 %all-to-all-done.2 = f32[8,2,96,1024]{3,2,1,0:T(8,128)} async-done(((f32[8,2,96,1024]{3,2,1,0:T(8,128)}), f32[8,2,96,1024]{3,2,1,0:T(8,128)}, u32[]{:S(2)}, u32[]{:S(2)}) %all-to-all-start.2) | async-done | bytes 6291488 | tf_op jit(solution)/shard_map/all_to_all | solution.py:105
  279.1 5.6 %gather_fusion.3 = f32[512,1024]{1,0:T(8,128)S(1)} fusion(f32[1536,1024]{1,0:T(8,128)} %bitcast.11, s32[1024]{0:T(1024)S(1)} %pad_clamp_fusion.2), kind=kCustom, calls=%fused_computation.3 | custom fusion | bytes 4196352 | tf_op jit(solution)/shard_map/gather | solution.py:112
  284.7 2.3 gather.24
  287.0 4.1 %select_reduce_fusion = f32[256,1024]{1,0:T(8,128)S(1)} fusion(f32[256,2,1024]{2,1,0:T(2,128)} %gather.24, pred[256,2]{1,0:T(8,128)(4,1)S(1)} %and.17), kind=kLoop, calls=%fused_computation.9 | loop fusion | flops 786432 | bytes 3146240 | tf_op jit(solution)/shard_map/reduce_sum | solution.py:115
  291.2 25.5 %all-reduce.2 = (bf16[256,1024]{1,0:T(8,128)(2,1)}, f32[512]{0:T(512)S(1)}) all-reduce(f32[256,1024]{1,0:T(8,128)S(1)} %select_reduce_fusion, f32[512]{0:T(512)S(1)} %get-tuple-element.26), channel_id=1, replica_groups=mesh['ep'=8,'tp'=4] {'tp'}, use_global_device_ids=true, to_apply=%region_6.7 | all-reduce | flops 262656 | bytes 1576960 | tf_op jit(solution)/shard_map/psum | solution.py:116
  (55 shorter events, 6.1 us)
Async XLA Ops:
  7.2 88.7 %copy-start = (bf16[2,1024,128]{2,1,0:T(8,128)(2,1)S(1)}, bf16[2,1024,128]{2,1,0:T(8,128)(2,1)}, u32[]{:S(2)}) copy-start(bf16[2,1024,128]{2,1,0:T(8,128)(2,1)} %param.11) | copy-start | bytes 1572868
  7.2 84.6 %all-gather.5.cloned.1.call-start = ((), (), s32[]{:S(2)}) async-start(), calls=%async_computation.5 | async-start | bytes 3932160 | tf_op jit(solution)/shard_map/all_gather | solution.py:88
  16.9 9.7 %copy-start.1 = (bf16[256,1024]{1,0:T(8,128)(2,1)S(1)}, bf16[256,1024]{1,0:T(8,128)(2,1)}, u32[]{:S(2)}) copy-start(bf16[256,1024]{1,0:T(8,128)(2,1)} %param.7) | copy-start | bytes 1572868
  32.3 28.9 %copy-start.2 = (bf16[256,1024]{1,0:T(8,128)(2,1)S(1)}, bf16[256,1024]{1,0:T(8,128)(2,1)}, u32[]{:S(2)}) copy-start(bf16[256,1024]{1,0:T(8,128)(2,1)} %param.8) | copy-start | bytes 1572868
  61.1 58.3 %all-gather.3.cloned.1.call-start = ((), (), s32[]{:S(2)}) async-start(), calls=%async_computation.4 | async-start | bytes 3932160 | tf_op jit(solution)/shard_map/all_gather | solution.py:89
  91.8 2.4 copy-start.7
  94.2 1.7 copy-start.3
  119.5 2.4 copy-start.8
  121.8 1.7 copy-start.5
  124.2 12.0 %all-to-all-start.3 = ((f32[8,2,96]{2,1,0:T(2,128)}), f32[8,2,96]{2,1,0:T(2,128)S(1)}, u32[]{:S(2)}, u32[]{:S(2)}) async-start(f32[8,2,96]{2,1,0:T(2,128)} %copy.74), calls=%async_computation.3 | async-start | bytes 16384 | tf_op jit(solution)/shard_map/all_to_all | solution.py:106
  136.2 142.9 %all-to-all-start.2 = ((f32[8,2,96,1024]{3,2,1,0:T(8,128)}), f32[8,2,96,1024]{3,2,1,0:T(8,128)}, u32[]{:S(2)}, u32[]{:S(2)}) async-start(f32[8,2,96,1024]{3,2,1,0:T(8,128)} %bitcast.50), calls=%async_computation.2 | async-start | bytes 12582912 | tf_op jit(solution)/shard_map/all_to_all | solution.py:105
  141.1 4.4 %copy-start.6 = (bf16[2,8,96,1024]{3,2,1,0:T(8,128)(2,1)S(1)}, bf16[2,8,96,1024]{3,2,1,0:T(8,128)(2,1)}, u32[]{:S(2)}) copy-start(bf16[2,8,96,1024]{3,2,1,0:T(8,128)(2,1)} %copy-done.5) | copy-start | bytes 9437188
  145.4 2.2 copy-start.4
Sparse Core Ops, SparseCore 0:
  61.2 27.5 all-gather.4
  91.9 27.4 all-gather.2
where the time goes:
time: 325 us; the launch traced here: 324 us
  waiting for transfers between devices  149 us (46%)
  blocking collectives  76.2 us (23%)
  local copies, waits for them, and re-layouts  50.8 us (16%)
  between operations  14.4 us (4%)
  matrix products  14.3 us (4%)
  starting transfers between devices  10.4 us (3%)
  other arithmetic  8.97 us (3%)
    all_to_all x1, waiting for transfers between devices, shards(): lax.all_to_all(input_grad, 'ep', split_axis=0, concat_axis=0, tiled=True)  126 us
    all_to_all x1, blocking collectives, shards(): lax.all_to_all(part_rows, 'ep', split_axis=0, concat_axis=0, tiled=True)  27.4 us
    psum x1, blocking collectives, shards(): total_grad, total_product = lax.psum((token_grad, pair_product), 'tp')  25.5 us
    all_to_all x1, blocking collectives, shards(): lax.all_to_all(part_scaled, 'ep', split_axis=0, concat_axis=0, tiled=True)  23.2 us
    all_gather x1, waiting for transfers between devices, shards(): lax.all_gather(landed[1], 'tp', axis=2, tiled=True)  22.4 us
    gather x1, local copies, waits for them, and re-layouts, shards(): gate_weights.reshape(pair_count)[owner_pair]  9.48 us
    gather x2, local copies, waits for them, and re-layouts, shards(): back_grad.reshape(experts * capacity, model_width)[back_index]  7.9 us
  transfers between devices with their start and end apart: 4, of which 3 were waited for; matrix products, arithmetic and copies ran while one was open for 9% of the time, Pallas kernels for 0%

commit v1 on v0

--- a/solution.py
+++ b/solution.py
@@ -2,6 +2,11 @@
 import jax.numpy as jnp
 from jax import lax
 from jax.sharding import PartitionSpec as P
+
+
+def gather_blocks(block, mesh_axis, dim):
+    pieces = lax.all_gather(block, mesh_axis)
+    return jnp.concatenate(pieces, axis=dim)
 
 
 def expert_terms(expert_rows, expert_scaled, gate_proj, up_proj, down_proj):
@@ -86,7 +91,7 @@
     )
     recv_rows, recv_scaled = (
         lax.all_gather(landed[0], "tp", axis=2, tiled=True),
-        lax.all_gather(landed[1], "tp", axis=2, tiled=True),
+        gather_blocks(landed[1], "tp", 2),
     )
     expert_rows = recv_rows.transpose(1, 0, 2, 3).reshape(
         local_experts, groups * capacity, model_width

time: 325 us -> 325 us (level)
  no operation moved by 1% of the time
where the time goes in v1:
time: 325 us; the launch traced here: 324 us
  waiting for transfers between devices  149 us (46%)
  blocking collectives  76.1 us (23%)
  local copies, waits for them, and re-layouts  50.8 us (16%)
  between operations  14.4 us (4%)
  matrix products  14.3 us (4%)
  starting transfers between devices  10.4 us (3%)
  other arithmetic  8.97 us (3%)
    all_to_all x1, waiting for transfers between devices, shards(): lax.all_to_all(input_grad, 'ep', split_axis=0, concat_axis=0, tiled=True)  126 us
    all_to_all x1, blocking collectives, shards(): lax.all_to_all(part_rows, 'ep', split_axis=0, concat_axis=0, tiled=True)  27.4 us
    psum x1, blocking collectives, shards(): total_grad, total_product = lax.psum((token_grad, pair_product), 'tp')  25.5 us
    all_to_all x1, blocking collectives, shards(): lax.all_to_all(part_scaled, 'ep', split_axis=0, concat_axis=0, tiled=True)  23.2 us
    all_gather x1, waiting for transfers between devices, gather_blocks(): pieces = lax.all_gather(block, mesh_axis)  22.4 us
    gather x1, local copies, waits for them, and re-layouts, shards(): gate_weights.reshape(pair_count)[owner_pair]  9.48 us
    gather x2, local copies, waits for them, and re-layouts, shards(): back_grad.reshape(experts * capacity, model_width)[back_index]  7.9 us
  transfers between devices with their start and end apart: 4, of which 3 were waited for; matrix products, arithmetic and copies ran while one was open for 9% of the time, Pallas kernels for 0%

profile of v1, /device:TPU:0, one launch (start us, length us, event | category | flops | bytes accessed | tf_op | source)
XLA Modules:
  0.0 324.4 jit_solution(9123249410228681387)
XLA Ops:
  9.4 1.2 reduce-window.6
  10.9 2.5 scatter_custom_fusion.1
  13.4 2.5 scatter_custom_fusion
  15.9 0.8 copy.64
  16.9 9.5 %gather_fusion = f32[1536]{0:T(1024)S(1)} fusion(f32[512]{0:T(512)S(1)} %reshape.154, s32[2048]{0:T(1024)S(1)} %get-tuple-element.38), kind=kCustom, calls=%fused_computation | custom fusion | bytes 18432 | tf_op jit(solution)/shard_map/gather | solution.py:76
  26.5 5.8 %gather_fusion.2 = bf16[1536,1024]{1,0:T(8,128)(2,1)} fusion(bf16[256,1024]{1,0:T(8,128)(2,1)S(1)} %copy-done.1, s32[2048]{0:T(1024)S(1)} %get-tuple-element.37), kind=kCustom, calls=%fused_computation.2 | custom fusion | bytes 6297600 | tf_op jit(solution)/shard_map/gather | solution.py:77
  32.3 1.4 dynamic-slice_select_fusion
  33.7 27.4 %all_to_all.20 = bf16[8,2,24,1024]{3,2,1,0:T(8,128)(2,1)} all-to-all(bf16[8,2,24,1024]{3,2,1,0:T(8,128)(2,1)S(1)} %dynamic-slice_select_fusion), channel_id=1, replica_groups=mesh['ep'=8,'tp'=4] {'ep'}, dimensions={0} | all-to-all | bytes 1572864 | tf_op jit(solution)/shard_map/all_to_all | solution.py:89
  61.3 5.8 %gather_fusion.1 = bf16[1536,1024]{1,0:T(8,128)(2,1)} fusion(bf16[256,1024]{1,0:T(8,128)(2,1)S(1)} %copy-done.2, s32[2048]{0:T(1024)S(1)} %get-tuple-element.37), kind=kCustom, calls=%fused_computation.1 | custom fusion | bytes 6297600 | tf_op jit(solution)/shard_map/gather | solution.py:78
  67.1 1.4 fusion
  68.5 23.2 %all_to_all.21 = bf16[8,2,24,1024]{3,2,1,0:T(8,128)(2,1)} all-to-all(bf16[8,2,24,1024]{3,2,1,0:T(8,128)(2,1)S(1)} %fusion), channel_id=1, replica_groups=mesh['ep'=8,'tp'=4] {'ep'}, dimensions={0} | all-to-all | bytes 1572864 | tf_op jit(solution)/shard_map/all_to_all | solution.py:90
  91.8 2.4 copy.66
  94.2 1.2 convolution_convert_fusion
  95.9 1.2 convolution_convert_fusion.1
  97.1 22.4 %all-gather.6.cloned.1.call-done = bf16[32,2,24,1024]{3,2,1,0:T(8,128)(2,1)} async-done(((bf16[8,2,24,1024]{3,2,1,0:T(8,128)(2,1)}), bf16[32,2,24,1024]{3,2,1,0:T(8,128)(2,1)}) %all-gather.6.cloned.1.call-update) | async-done | bytes 3145744 | tf_op jit(solution)/shard_map/all_gather | solution.py:8
  119.5 2.4 copy.65
  121.9 1.4 multiply_reduce_fusion
  124.2 5.5 %all-to-all-start.3 = ((f32[8,2,96]{2,1,0:T(2,128)}), f32[8,2,96]{2,1,0:T(2,128)S(1)}, u32[]{:S(2)}, u32[]{:S(2)}) async-start(f32[8,2,96]{2,1,0:T(2,128)} %copy.72), calls=%async_computation.3 | async-start | bytes 16384 | tf_op jit(solution)/shard_map/all_to_all | solution.py:111
  129.7 1.0 fusion.21
  130.8 1.1 convolution_add_fusion
  131.8 3.2 copy.89
  135.1 1.2 all-to-all-done.3
  136.2 4.8 %all-to-all-start.2 = ((f32[8,2,96,1024]{3,2,1,0:T(8,128)}), f32[8,2,96,1024]{3,2,1,0:T(8,128)}, u32[]{:S(2)}, u32[]{:S(2)}) async-start(f32[8,2,96,1024]{3,2,1,0:T(8,128)} %bitcast.56), calls=%async_computation.2 | async-start | bytes 12582912 | tf_op jit(solution)/shard_map/all_to_all | solution.py:110
  141.1 4.4 %fusion.22 = f32[2,1024,128]{2,1,0:T(8,128)} fusion(bf16[2,768,1024]{2,1,0:T(8,128)(2,1)} %bitcast.54, bf16[2,768,128]{1,2,0:T(8,128)(2,1)S(1)} %get-tuple-element.31), kind=kOutput, calls=%fused_computation.67 | convolution fusion | flops 402653184 | bytes 4587520 | tf_op jit(solution)/shard_map/erd,erf->edf/dot_general | solution.py:45
  145.5 1.8 fusion.9
  147.7 2.4 fusion.20
  150.1 3.1 gather_fusion.4
  153.5 125.7 %all-to-all-done.2 = f32[8,2,96,1024]{3,2,1,0:T(8,128)} async-done(((f32[8,2,96,1024]{3,2,1,0:T(8,128)}), f32[8,2,96,1024]{3,2,1,0:T(8,128)}, u32[]{:S(2)}, u32[]{:S(2)}) %all-to-all-start.2) | async-done | bytes 6291488 | tf_op jit(solution)/shard_map/all_to_all | solution.py:110
  279.1 5.6 %gather_fusion.3 = f32[512,1024]{1,0:T(8,128)S(1)} fusion(f32[1536,1024]{1,0:T(8,128)} %bitcast.14, s32[1024]{0:T(1024)S(1)} %pad_clamp_fusion.2), kind=kCustom, calls=%fused_computation.3 | custom fusion | bytes 4196352 | tf_op jit(solution)/shard_map/gather | solution.py:117
  284.8 2.3 gather.24
  287.0 4.1 %select_reduce_fusion = f32[256,1024]{1,0:T(8,128)S(1)} fusion(f32[256,2,1024]{2,1,0:T(2,128)} %gather.24, pred[256,2]{1,0:T(8,128)(4,1)S(1)} %and.17), kind=kLoop, calls=%fused_computation.9 | loop fusion | flops 786432 | bytes 3146240 | tf_op jit(solution)/shard_map/reduce_sum | solution.py:120
  291.2 25.5 %all-reduce.2 = (bf16[256,1024]{1,0:T(8,128)(2,1)}, f32[512]{0:T(512)S(1)}) all-reduce(f32[256,1024]{1,0:T(8,128)S(1)} %select_reduce_fusion, f32[512]{0:T(512)S(1)} %get-tuple-element.26), channel_id=1, replica_groups=mesh['ep'=8,'tp'=4] {'tp'}, use_global_device_ids=true, to_apply=%region_6.7 | all-reduce | flops 262656 | bytes 1576960 | tf_op jit(solution)/shard_map/psum | solution.py:121
  (55 shorter events, 6.1 us)
Async XLA Ops:
  7.2 88.7 %copy-start = (bf16[2,1024,128]{2,1,0:T(8,128)(2,1)S(1)}, bf16[2,1024,128]{2,1,0:T(8,128)(2,1)}, u32[]{:S(2)}) copy-start(bf16[2,1024,128]{2,1,0:T(8,128)(2,1)} %param.11) | copy-start | bytes 1572868
  7.2 84.6 %all-gather.4.cloned.1.call-start = ((), (), s32[]{:S(2)}) async-start(), calls=%async_computation.4 | async-start | bytes 3932160 | tf_op jit(solution)/shard_map/all_gather | solution.py:93
  16.9 9.7 %copy-start.1 = (bf16[256,1024]{1,0:T(8,128)(2,1)S(1)}, bf16[256,1024]{1,0:T(8,128)(2,1)}, u32[]{:S(2)}) copy-start(bf16[256,1024]{1,0:T(8,128)(2,1)} %param.7) | copy-start | bytes 1572868
  32.3 28.9 %copy-start.2 = (bf16[256,1024]{1,0:T(8,128)(2,1)S(1)}, bf16[256,1024]{1,0:T(8,128)(2,1)}, u32[]{:S(2)}) copy-start(bf16[256,1024]{1,0:T(8,128)(2,1)} %param.8) | copy-start | bytes 1572868
  61.1 58.3 %all-gather.6.cloned.1.call-start = ((), (), s32[]{:S(2)}) async-start(), calls=%async_computation.5 | async-start | bytes 3932160 | tf_op jit(solution)/shard_map/all_gather | solution.py:8
  91.8 2.4 copy-start.7
  94.2 1.7 copy-start.3
  119.5 2.4 copy-start.8
  121.9 1.7 copy-start.5
  124.2 12.0 %all-to-all-start.3 = ((f32[8,2,96]{2,1,0:T(2,128)}), f32[8,2,96]{2,1,0:T(2,128)S(1)}, u32[]{:S(2)}, u32[]{:S(2)}) async-start(f32[8,2,96]{2,1,0:T(2,128)} %copy.72), calls=%async_computation.3 | async-start | bytes 16384 | tf_op jit(solution)/shard_map/all_to_all | solution.py:111
  136.2 142.9 %all-to-all-start.2 = ((f32[8,2,96,1024]{3,2,1,0:T(8,128)}), f32[8,2,96,1024]{3,2,1,0:T(8,128)}, u32[]{:S(2)}, u32[]{:S(2)}) async-start(f32[8,2,96,1024]{3,2,1,0:T(8,128)} %bitcast.56), calls=%async_computation.2 | async-start | bytes 12582912 | tf_op jit(solution)/shard_map/all_to_all | solution.py:110
  141.1 4.4 %copy-start.6 = (bf16[8,2,4,24,1024]{4,3,2,0,1:T(8,128)(2,1)S(1)}, bf16[8,2,4,24,1024]{4,3,2,0,1:T(8,128)(2,1)}, u32[]{:S(2)}) copy-start(bf16[8,2,4,24,1024]{4,3,2,0,1:T(8,128)(2,1)} %copy-done.5) | copy-start | bytes 9437188
  145.5 2.2 copy-start.4
Sparse Core Ops, SparseCore 0:
  61.2 27.5 all-gather.3
  91.9 27.4 all-gather.5
